TPU v7x, 32 devices: a whole 2x2x4 slice. The times are simulated.
32 devices in a mesh: kv: 8 (over z, y), tp: 4 (over x, core).
Axes of the slice: x: 2, y: 2, z: 4, core: 2. Of those that a mesh axis runs over, the one named last changes fastest.
Arguments:
- tokens: bfloat16 [128, 4096], P('tp', 'kv')
- seq_pos: int32 [128], P('kv'), may hold values from 0 to 4095
- state: float32 [128, 16, 128, 256], P('kv', 'tp'), may hold values from -0.6 to 0.6
- norm_in_gain: float32 [4096], P('kv'), may hold values from 0.1 to 1.9
- query_weight: bfloat16 [4096, 2048], P('kv', 'tp'), may hold values from -0.09375 to 0.09375
- key_weight: bfloat16 [4096, 2048], P('kv', 'tp'), may hold values from -0.09375 to 0.09375
- value_weight: bfloat16 [4096, 4096], P('kv', 'tp'), may hold values from -0.09375 to 0.09375
- gate_weight: bfloat16 [4096, 4096], P('kv', 'tp'), may hold values from -0.09375 to 0.09375
- head_gain: float32 [4096], P('tp'), may hold values from 0.1 to 1.9
- out_weight: bfloat16 [4096, 4096], P('tp', 'kv'), may hold values from -0.09375 to 0.09375
- norm_mlp_gain: float32 [4096], P('kv'), may hold values from 0.1 to 1.9
- hidden_weight: bfloat16 [4096, 16384], P('kv', 'tp'), may hold values from -0.09375 to 0.09375
- down_weight: bfloat16 [16384, 4096], P('tp', 'kv'), may hold values from -0.046875 to 0.046875
Outputs:
- output: bfloat16 [128, 4096], P('tp', 'kv')
- new_state: float32 [128, 16, 128, 256], P('kv', 'tp')
All inputs are finite; a program needn't handle non-finite values.
Results may differ from a plain program's by a relative error of at most 0.03.
Values may be sent and summed in bfloat16 or wider, within the bound.
A program may use at most 64 MiB of HBM per device.

v0:
```python
import jax
import jax.numpy as jnp
from jax import lax
from jax.sharding import PartitionSpec as P

D = 4096
H = 16
DK = 128
DV = 256
EPS = 1e-06


def rotate(vectors, positions):
    half = vectors.shape[-1] // 2
    inverse = jnp.power(10000.0, -jnp.arange(half, dtype=jnp.float32) / half)
    angles = positions.astype(jnp.float32)[:, None] * inverse[None, :]
    cosine = jnp.cos(angles)[:, None, :]
    sine = jnp.sin(angles)[:, None, :]
    first, second = (vectors[..., :half], vectors[..., half:])
    return jnp.concatenate(
        [first * cosine - second * sine, first * sine + second * cosine], axis=-1
    )


def head_decay(head_ids):
    return 1.0 - jnp.exp2(-2.0 - 6.0 * head_ids / (H - 1))


def local(
    tokens,
    seq_pos,
    state,
    norm_in_gain,
    query_weight,
    key_weight,
    value_weight,
    gate_weight,
    head_gain,
    out_weight,
    norm_mlp_gain,
    hidden_weight,
    down_weight,
):
    rows_all = lax.all_gather(tokens, "tp", axis=0, tiled=True)
    rows_f = rows_all.astype(jnp.float32)
    squares_in = jnp.sum(rows_f * rows_f, axis=1)
    normed_in = (rows_f * norm_in_gain[None, :]).astype(jnp.bfloat16)
    term_query = jnp.dot(normed_in, query_weight, preferred_element_type=jnp.float32).astype(
        jnp.bfloat16
    )
    term_keys = jnp.dot(normed_in, key_weight, preferred_element_type=jnp.float32).astype(
        jnp.bfloat16
    )
    term_values = jnp.dot(normed_in, value_weight, preferred_element_type=jnp.float32).astype(
        jnp.bfloat16
    )
    term_gates = jnp.dot(normed_in, gate_weight, preferred_element_type=jnp.float32).astype(
        jnp.bfloat16
    )
    total_all = lax.psum(squares_in, "kv")
    query, keys, values, gates = (
        lax.psum_scatter(term_query, "kv", scatter_dimension=0, tiled=True).astype(jnp.float32),
        lax.psum_scatter(term_keys, "kv", scatter_dimension=0, tiled=True).astype(jnp.float32),
        lax.psum_scatter(term_values, "kv", scatter_dimension=0, tiled=True).astype(jnp.float32),
        lax.psum_scatter(term_gates, "kv", scatter_dimension=0, tiled=True).astype(jnp.float32),
    )
    own_rows = query.shape[0]
    total_in = lax.dynamic_slice_in_dim(total_all, lax.axis_index("kv") * own_rows, own_rows, 0)
    factor = lax.rsqrt(total_in / D + EPS)[:, None]
    query, keys, values, gates = (query * factor, keys * factor, values * factor, gates * factor)
    local_rows = query.shape[0]
    heads_dev = H // lax.axis_size("tp")
    turned_query = rotate(query.reshape(local_rows, heads_dev, DK), seq_pos)
    turned_keys = rotate(keys.reshape(local_rows, heads_dev, DK), seq_pos) * DK ** (-0.5)
    head_ids = (lax.axis_index("tp") * heads_dev + jnp.arange(heads_dev, dtype=jnp.int32)).astype(
        jnp.float32
    )
    decay = head_decay(head_ids)
    new_state = decay[None, :, None, None] * state + jnp.einsum(
        "bhk,bhv->bhkv",
        turned_keys,
        values.reshape(local_rows, heads_dev, DV),
        precision=lax.Precision.HIGHEST,
    )
    read = jnp.einsum("bhk,bhkv->bhv", turned_query, new_state, precision=lax.Precision.HIGHEST)
    read = read * lax.rsqrt(jnp.mean(read * read, axis=-1, keepdims=True) + EPS)
    mixed = (
        read.reshape(local_rows, heads_dev * DV) * head_gain[None, :] * jax.nn.silu(gates)
    ).astype(jnp.bfloat16)
    attn_terms = jnp.dot(
        lax.all_gather(mixed, "kv", axis=0, tiled=True),
        out_weight,
        preferred_element_type=jnp.float32,
    )
    attn = lax.psum_scatter(
        attn_terms.astype(jnp.bfloat16), "tp", scatter_dimension=0, tiled=True
    ).astype(jnp.float32)
    resid = (tokens.astype(jnp.float32) + attn).astype(jnp.bfloat16)
    resid_all = lax.all_gather(resid, "tp", axis=0, tiled=True)
    resid_f = resid_all.astype(jnp.float32)
    squares_mid = jnp.sum(resid_f * resid_f, axis=1)
    normed_mid = (resid_f * norm_mlp_gain[None, :]).astype(jnp.bfloat16)
    term_hidden = jnp.dot(normed_mid, hidden_weight, preferred_element_type=jnp.float32).astype(
        jnp.bfloat16
    )
    total_mid = lax.psum(squares_mid, "kv")
    scale_mid = lax.rsqrt(total_mid / D + EPS)[:, None]
    hidden = lax.psum(term_hidden, "kv").astype(jnp.float32)
    active = jnp.square(jax.nn.relu(hidden * scale_mid)).astype(jnp.bfloat16)
    down_terms = jnp.dot(active, down_weight, preferred_element_type=jnp.float32)
    down = lax.psum_scatter(
        down_terms.astype(jnp.bfloat16), "tp", scatter_dimension=0, tiled=True
    ).astype(jnp.float32)
    output = (resid.astype(jnp.float32) + down).astype(jnp.bfloat16)
    return (output, new_state)


def solution(mesh):
    placed = (
        P("tp", "kv"),
        P("kv"),
        P("kv", "tp", None, None),
        P("kv"),
        P("kv", "tp"),
        P("kv", "tp"),
        P("kv", "tp"),
        P("kv", "tp"),
        P("tp"),
        P("tp", "kv"),
        P("kv"),
        P("kv", "tp"),
        P("tp", "kv"),
    )
    return jax.shard_map(
        local,
        mesh=mesh,
        in_specs=placed,
        out_specs=(P("tp", "kv"), P("kv", "tp", None, None)),
        check_vma=False,
    )
```

profile of v0, /device:TPU:0, one launch (start us, length us, event | category | flops | bytes accessed | tf_op | source)
XLA Modules:
  0.0 445.5 jit_solution(3664040884219889815)
XLA Ops:
  7.2 6.9 %all_gather.9 = bf16[128,512]{1,0:T(8,128)(2,1)S(1)} all-gather(bf16[32,512]{1,0:T(8,128)(2,1)} %param.13), channel_id=1, replica_groups=mesh['kv'=8,'tp'=4] {'tp'}, dimensions={0}, use_global_device_ids=true | all-gather | bytes 163840 | tf_op jit(solution)/shard_map/all_gather | solution.py:44
  14.1 2.0 convolution_convert_fusion.4
  16.1 1.9 convolution_convert_fusion.5
  18.1 1.7 convolution_convert_fusion.2
  19.9 2.2 convolution_convert_fusion.1
  22.4 22.1 %psum.21 = f32[128]{0:T(128)S(1)} all-reduce(f32[128]{0:T(128)S(1)} %fusion.3), channel_id=1, replica_groups=mesh['kv'=8,'tp'=4] {'kv'}, use_global_device_ids=true, to_apply=%region_2.0 | all-reduce | flops 128 | bytes 1024 | tf_op jit(solution)/shard_map/psum | solution.py:60
  44.7 35.0 %reduce-scatter.9.cloned.1.call-done = bf16[16,512]{1,0:T(8,128)(2,1)} async-done(((bf16[128,512]{1,0:T(8,128)(2,1)}), bf16[16,512]{1,0:T(8,128)(2,1)}) %reduce-scatter.9.cloned.1.call-update) | async-done | bytes 16400 | tf_op jit(solution)/shard_map/reduce_scatter | solution.py:63
  79.7 64.2 %reduce-scatter.7.cloned.1.call-done = bf16[16,512]{1,0:T(8,128)(2,1)} async-done(((bf16[128,512]{1,0:T(8,128)(2,1)}), bf16[16,512]{1,0:T(8,128)(2,1)}) %reduce-scatter.7.cloned.1.call-update) | async-done | bytes 16400 | tf_op jit(solution)/shard_map/reduce_scatter | solution.py:62
  144.9 64.0 %reduce-scatter.11.cloned.1.call-done = bf16[16,1024]{1,0:T(8,128)(2,1)} async-done(((bf16[128,1024]{1,0:T(8,128)(2,1)}), bf16[16,1024]{1,0:T(8,128)(2,1)}) %reduce-scatter.11.cloned.1.call-update) | async-done | bytes 32784 | tf_op jit(solution)/shard_map/reduce_scatter | solution.py:64
  208.9 0.8 convert_multiply_fusion.4
  209.7 4.1 multiply_add_fusion
  213.9 4.1 fusion.14
  218.3 55.3 %reduce-scatter.13.cloned.1.call-done = bf16[16,1024]{1,0:T(8,128)(2,1)} async-done(((bf16[128,1024]{1,0:T(8,128)(2,1)}), bf16[16,1024]{1,0:T(8,128)(2,1)}) %reduce-scatter.13.cloned.1.call-update) | async-done | bytes 32784 | tf_op jit(solution)/shard_map/reduce_scatter | solution.py:65
  273.6 0.9 multiply_convert_fusion.2
  274.4 30.9 %all_gather.10 = bf16[128,1024]{1,0:T(8,128)(2,1)S(1)} all-gather(bf16[16,1024]{1,0:T(8,128)(2,1)S(1)} %multiply_convert_fusion.2), channel_id=1, replica_groups=mesh['kv'=8,'tp'=4] {'kv'}, dimensions={0}, use_global_device_ids=true | all-gather | bytes 294912 | tf_op jit(solution)/shard_map/all_gather | solution.py:91
  305.3 1.0 convolution_convert_fusion.6
  306.4 18.8 %reduce-scatter.15.cloned.1.call-done = bf16[32,512]{1,0:T(8,128)(2,1)} async-done(((bf16[128,512]{1,0:T(8,128)(2,1)}), bf16[32,512]{1,0:T(8,128)(2,1)}) %reduce-scatter.15.cloned.1.call-update) | async-done | bytes 32784 | tf_op jit(solution)/shard_map/reduce_scatter | solution.py:95
  325.9 5.4 %all_gather.11 = bf16[128,512]{1,0:T(8,128)(2,1)S(1)} all-gather(bf16[32,512]{1,0:T(8,128)(2,1)S(1)} %add_convert_fusion.1), channel_id=1, replica_groups=mesh['kv'=8,'tp'=4] {'tp'}, dimensions={0}, use_global_device_ids=true | all-gather | bytes 163840 | tf_op jit(solution)/shard_map/all_gather | solution.py:99
  331.3 3.9 convolution_convert_fusion
  335.5 21.6 %psum.23 = f32[128]{0:T(128)S(1)} all-reduce(f32[128]{0:T(128)S(1)} %fusion.5), channel_id=1, replica_groups=mesh['kv'=8,'tp'=4] {'kv'}, use_global_device_ids=true, to_apply=%region_10.11 | all-reduce | flops 128 | bytes 1024 | tf_op jit(solution)/shard_map/psum | solution.py:106
  357.1 56.9 %all-reduce.2.cloned.1.call-done = bf16[128,4096]{1,0:T(8,128)(2,1)} async-done(((bf16[128,4096]{1,0:T(8,128)(2,1)}), bf16[128,4096]{1,0:T(8,128)(2,1)}) %all-reduce.2.cloned.1.call-update) | async-done | bytes 1048592 | tf_op jit(solution)/shard_map/psum | solution.py:108
  414.0 3.9 convolution_convert_fusion.3
  417.9 19.4 %reduce-scatter.17.cloned.1.call-done = bf16[32,512]{1,0:T(8,128)(2,1)} async-done(((bf16[128,512]{1,0:T(8,128)(2,1)}), bf16[32,512]{1,0:T(8,128)(2,1)}) %reduce-scatter.17.cloned.1.call-update) | async-done | bytes 32784 | tf_op jit(solution)/shard_map/reduce_scatter | solution.py:111
  437.3 1.4 add_convert_fusion
  (47 shorter events, 2.9 us)
Async XLA Ops:
  7.2 11.0 %copy-start = (bf16[512,1024]{1,0:T(8,128)(2,1)S(1)}, bf16[512,1024]{1,0:T(8,128)(2,1)}, u32[]{:S(2)}) copy-start(bf16[512,1024]{1,0:T(8,128)(2,1)} %param.19) | copy-start | bytes 3145732
  7.2 15.2 %copy-start.6 = (s32[16]{0:T(128)S(1)}, s32[16]{0:T(128)}, u32[]{:S(2)}) copy-start(s32[16]{0:T(128)} %param.14) | copy-start | bytes 196
  7.2 72.5 %reduce-scatter.9.cloned.1.call-start = ((), (), s32[]{:S(2)}) async-start(), calls=%async_computation.7 | async-start | bytes 147456 | tf_op jit(solution)/shard_map/reduce_scatter | solution.py:63
  16.1 127.8 %reduce-scatter.7.cloned.1.call-start = ((), (), s32[]{:S(2)}) async-start(), calls=%async_computation.6 | async-start | bytes 147456 | tf_op jit(solution)/shard_map/reduce_scatter | solution.py:62
  18.1 190.8 %reduce-scatter.11.cloned.1.call-start = ((), (), s32[]{:S(2)}) async-start(), calls=%async_computation.8 | async-start | bytes 294912 | tf_op jit(solution)/shard_map/reduce_scatter | solution.py:64
  19.9 253.7 %reduce-scatter.13.cloned.1.call-start = ((), (), s32[]{:S(2)}) async-start(), calls=%async_computation.9 | async-start | bytes 294912 | tf_op jit(solution)/shard_map/reduce_scatter | solution.py:65
  22.2 303.0 %reduce-scatter.15.cloned.1.call-start = ((), (), s32[]{:S(2)}) async-start(), calls=%async_computation.10 | async-start | bytes 163840 | tf_op jit(solution)/shard_map/reduce_scatter | solution.py:95
  213.9 4.1 copy-start.1
  213.9 59.7 %copy-start.4 = (f32[1024]{0:T(1024)S(1)}, f32[1024]{0:T(1024)}, u32[]{:S(2)}) copy-start(f32[1024]{0:T(1024)} %param.21) | copy-start | bytes 12292
  213.9 91.4 %copy-start.2 = (bf16[1024,512]{1,0:T(8,128)(2,1)S(1)}, bf16[1024,512]{1,0:T(8,128)(2,1)}, u32[]{:S(2)}) copy-start(bf16[1024,512]{1,0:T(8,128)(2,1)} %param.22) | copy-start | bytes 3145732
  213.9 111.2 %copy-start.3 = (bf16[32,512]{1,0:T(8,128)(2,1)S(1)}, bf16[32,512]{1,0:T(8,128)(2,1)}, u32[]{:S(2)}) copy-start(bf16[32,512]{1,0:T(8,128)(2,1)} %param.13) | copy-start | bytes 98308
  213.9 117.4 %copy-start.5 = (f32[512]{0:T(512)S(1)}, f32[512]{0:T(512)}, u32[]{:S(2)}) copy-start(f32[512]{0:T(512)} %param.23) | copy-start | bytes 6148
  306.3 107.6 %all-reduce.2.cloned.1.call-start = ((), (), s32[]{:S(2)}) async-start(), calls=%async_computation.11 | async-start | bytes 2097152 | tf_op jit(solution)/shard_map/psum | solution.py:108
  335.3 102.0 %reduce-scatter.17.cloned.1.call-start = ((), (), s32[]{:S(2)}) async-start(), calls=%async_computation.12 | async-start | bytes 163840 | tf_op jit(solution)/shard_map/reduce_scatter | solution.py:111
Sparse Core Ops, SparseCore 0:
  16.2 63.4 reduce-scatter.8
  83.0 60.8 reduce-scatter.6
  147.8 61.0 reduce-scatter.10
  212.1 61.4 reduce-scatter.12
  306.5 18.6 reduce-scatter.14
  335.4 78.4 all-reduce.1
  418.0 19.2 reduce-scatter.16
where the time goes:
time: 446 us
  waiting for transfers between devices  314 us (70%)
  blocking collectives  86.9 us (19%)
  matrix products  20.8 us (5%)
  between operations  14.3 us (3%)
  other arithmetic  9.62 us (2%)
    reduce_scatter x1, waiting for transfers between devices, local(): lax.psum_scatter(term_query, 'kv', scatter_dimension=0, tiled=True)  64.2 us
    reduce_scatter x1, waiting for transfers between devices, local(): lax.psum_scatter(term_values, 'kv', scatter_dimension=0, tiled=True)  64 us
    psum x1, waiting for transfers between devices, local(): hidden = lax.psum(term_hidden, 'kv').astype(jnp.float32)  56.9 us
    reduce_scatter x1, waiting for transfers between devices, local(): lax.psum_scatter(term_gates, 'kv', scatter_dimension=0, tiled=True)  55.3 us
    reduce_scatter x1, waiting for transfers between devices, local(): lax.psum_scatter(term_keys, 'kv', scatter_dimension=0, tiled=True)  35 us
    all_gather x1, blocking collectives, local(): lax.all_gather(mixed, 'kv', axis=0, tiled=True)  30.9 us
    psum x1, blocking collectives, local(): total_all = lax.psum(squares_in, 'kv')  22.1 us
    psum x1, blocking collectives, local(): total_mid = lax.psum(squares_mid, 'kv')  21.6 us
  transfers between devices with their start and end apart: 7, of which 7 were waited for; matrix products, arithmetic and copies ran while one was open for 4% of the time, Pallas kernels for 0%

commit v1 on v0

--- a/solution.py
+++ b/solution.py
@@ -105,7 +105,7 @@
     )
     total_mid = lax.psum(squares_mid, "kv")
     scale_mid = lax.rsqrt(total_mid / D + EPS)[:, None]
-    hidden = lax.psum(term_hidden, "kv").astype(jnp.float32)
+    hidden = jnp.sum(lax.all_gather(term_hidden, "kv"), axis=0).astype(jnp.float32)
     active = jnp.square(jax.nn.relu(hidden * scale_mid)).astype(jnp.bfloat16)
     down_terms = jnp.dot(active, down_weight, preferred_element_type=jnp.float32)
     down = lax.psum_scatter(

time: 446 us -> 496 us (1.11)
  waiting for transfers between devices: 314 us -> 358 us
    all_gather x0 -> x1, waiting for transfers between devices: none -> 103 us  [local(): lax.all_gather(term_hidden, 'kv')]
    psum x1 -> x0, waiting for transfers between devices: 56.9 us -> none  [local(): hidden = lax.psum(term_hidden, 'kv').astype(jnp.float32)]
  transfers between devices with their start and end apart: 7 -> 7, of which waited for: 7 -> 7; matrix products, arithmetic and copies ran while one was open for 4% -> 3% of each run, Pallas kernels for 0% -> 0%
where the time goes in v1:
time: 496 us; the launch traced here: 495 us
  waiting for transfers between devices  358 us (72%)
  blocking collectives  87.2 us (18%)
  matrix products  20.5 us (4%)
  other arithmetic  14.5 us (3%)
  between operations  14.3 us (3%)
    all_gather x1, waiting for transfers between devices, local(): lax.all_gather(term_hidden, 'kv')  103 us
    reduce_scatter x1, waiting for transfers between devices, local(): lax.psum_scatter(term_query, 'kv', scatter_dimension=0, tiled=True)  64.2 us
    reduce_scatter x1, waiting for transfers between devices, local(): lax.psum_scatter(term_values, 'kv', scatter_dimension=0, tiled=True)  64 us
    reduce_scatter x1, waiting for transfers between devices, local(): lax.psum_scatter(term_gates, 'kv', scatter_dimension=0, tiled=True)  55.3 us
    reduce_scatter x1, waiting for transfers between devices, local(): lax.psum_scatter(term_keys, 'kv', scatter_dimension=0, tiled=True)  35 us
    all_gather x1, blocking collectives, local(): lax.all_gather(mixed, 'kv', axis=0, tiled=True)  30.9 us
    psum x1, blocking collectives, local(): total_all = lax.psum(squares_in, 'kv')  22.1 us
    psum x1, blocking collectives, local(): total_mid = lax.psum(squares_mid, 'kv')  21.9 us
  transfers between devices with their start and end apart: 7, of which 7 were waited for; matrix products, arithmetic and copies ran while one was open for 3% of the time, Pallas kernels for 0%

profile of v1, /device:TPU:0, one launch (start us, length us, event | category | flops | bytes accessed | tf_op | source)
XLA Modules:
  0.0 494.9 jit_solution(8923346000337683022)
XLA Ops:
  7.2 6.9 %all_gather.15 = bf16[128,512]{1,0:T(8,128)(2,1)S(1)} all-gather(bf16[32,512]{1,0:T(8,128)(2,1)} %param.13), channel_id=1, replica_groups=mesh['kv'=8,'tp'=4] {'tp'}, dimensions={0}, use_global_device_ids=true | all-gather | bytes 163840 | tf_op jit(solution)/shard_map/all_gather | solution.py:44
  14.1 2.0 convolution_convert_fusion.4
  16.1 1.9 convolution_convert_fusion.5
  18.1 1.7 convolution_convert_fusion.2
  19.9 2.2 convolution_convert_fusion.1
  22.4 22.1 %psum.14 = f32[128]{0:T(128)S(1)} all-reduce(f32[128]{0:T(128)S(1)} %fusion.3), channel_id=1, replica_groups=mesh['kv'=8,'tp'=4] {'kv'}, use_global_device_ids=true, to_apply=%region_2.0 | all-reduce | flops 128 | bytes 1024 | tf_op jit(solution)/shard_map/psum | solution.py:60
  44.7 35.0 %reduce-scatter.9.cloned.1.call-done = bf16[16,512]{1,0:T(8,128)(2,1)} async-done(((bf16[128,512]{1,0:T(8,128)(2,1)}), bf16[16,512]{1,0:T(8,128)(2,1)}) %reduce-scatter.9.cloned.1.call-update) | async-done | bytes 16400 | tf_op jit(solution)/shard_map/reduce_scatter | solution.py:63
  79.7 64.2 %reduce-scatter.7.cloned.1.call-done = bf16[16,512]{1,0:T(8,128)(2,1)} async-done(((bf16[128,512]{1,0:T(8,128)(2,1)}), bf16[16,512]{1,0:T(8,128)(2,1)}) %reduce-scatter.7.cloned.1.call-update) | async-done | bytes 16400 | tf_op jit(solution)/shard_map/reduce_scatter | solution.py:62
  144.9 64.0 %reduce-scatter.11.cloned.1.call-done = bf16[16,1024]{1,0:T(8,128)(2,1)} async-done(((bf16[128,1024]{1,0:T(8,128)(2,1)}), bf16[16,1024]{1,0:T(8,128)(2,1)}) %reduce-scatter.11.cloned.1.call-update) | async-done | bytes 32784 | tf_op jit(solution)/shard_map/reduce_scatter | solution.py:64
  209.7 4.1 multiply_add_fusion
  213.9 4.1 fusion.14
  218.3 55.3 %reduce-scatter.13.cloned.1.call-done = bf16[16,1024]{1,0:T(8,128)(2,1)} async-done(((bf16[128,1024]{1,0:T(8,128)(2,1)}), bf16[16,1024]{1,0:T(8,128)(2,1)}) %reduce-scatter.13.cloned.1.call-update) | async-done | bytes 32784 | tf_op jit(solution)/shard_map/reduce_scatter | solution.py:65
  273.6 0.9 multiply_convert_fusion.2
  274.4 30.9 %all_gather.16 = bf16[128,1024]{1,0:T(8,128)(2,1)S(1)} all-gather(bf16[16,1024]{1,0:T(8,128)(2,1)S(1)} %multiply_convert_fusion.2), channel_id=1, replica_groups=mesh['kv'=8,'tp'=4] {'kv'}, dimensions={0}, use_global_device_ids=true | all-gather | bytes 294912 | tf_op jit(solution)/shard_map/all_gather | solution.py:91
  305.3 1.0 convolution_convert_fusion.6
  306.4 18.8 %reduce-scatter.15.cloned.1.call-done = bf16[32,512]{1,0:T(8,128)(2,1)} async-done(((bf16[128,512]{1,0:T(8,128)(2,1)}), bf16[32,512]{1,0:T(8,128)(2,1)}) %reduce-scatter.15.cloned.1.call-update) | async-done | bytes 32784 | tf_op jit(solution)/shard_map/reduce_scatter | solution.py:95
  325.9 5.4 %all_gather.17 = bf16[128,512]{1,0:T(8,128)(2,1)S(1)} all-gather(bf16[32,512]{1,0:T(8,128)(2,1)S(1)} %add_convert_fusion.1), channel_id=1, replica_groups=mesh['kv'=8,'tp'=4] {'tp'}, dimensions={0}, use_global_device_ids=true | all-gather | bytes 163840 | tf_op jit(solution)/shard_map/all_gather | solution.py:99
  331.3 4.0 convolution_convert_fusion
  335.5 21.9 %psum.15 = f32[128]{0:T(128)S(1)} all-reduce(f32[128]{0:T(128)S(1)} %fusion.5), channel_id=1, replica_groups=mesh['kv'=8,'tp'=4] {'kv'}, use_global_device_ids=true, to_apply=%region_10.11 | all-reduce | flops 128 | bytes 1024 | tf_op jit(solution)/shard_map/psum | solution.py:106
  357.5 102.6 %all-gather.3.cloned.1.call-done = bf16[1024,4096]{1,0:T(8,128)(2,1)} async-done(((bf16[128,4096]{1,0:T(8,128)(2,1)}), bf16[1024,4096]{1,0:T(8,128)(2,1)}) %all-gather.3.cloned.1.call-update) | async-done | bytes 8388624 | tf_op jit(solution)/shard_map/all_gather | solution.py:108
  460.1 4.9 reduce_sum.41
  465.0 3.6 convolution_convert_fusion.3
  468.6 18.0 %reduce-scatter.17.cloned.1.call-done = bf16[32,512]{1,0:T(8,128)(2,1)} async-done(((bf16[128,512]{1,0:T(8,128)(2,1)}), bf16[32,512]{1,0:T(8,128)(2,1)}) %reduce-scatter.17.cloned.1.call-update) | async-done | bytes 32784 | tf_op jit(solution)/shard_map/reduce_scatter | solution.py:111
  486.6 1.4 add_convert_fusion
  (48 shorter events, 3.8 us)
Async XLA Ops:
  7.2 11.0 %copy-start = (bf16[512,1024]{1,0:T(8,128)(2,1)S(1)}, bf16[512,1024]{1,0:T(8,128)(2,1)}, u32[]{:S(2)}) copy-start(bf16[512,1024]{1,0:T(8,128)(2,1)} %param.19) | copy-start | bytes 3145732
  7.2 15.2 %copy-start.6 = (s32[16]{0:T(128)S(1)}, s32[16]{0:T(128)}, u32[]{:S(2)}) copy-start(s32[16]{0:T(128)} %param.14) | copy-start | bytes 196
  7.2 72.5 %reduce-scatter.9.cloned.1.call-start = ((), (), s32[]{:S(2)}) async-start(), calls=%async_computation.7 | async-start | bytes 147456 | tf_op jit(solution)/shard_map/reduce_scatter | solution.py:63
  16.1 127.8 %reduce-scatter.7.cloned.1.call-start = ((), (), s32[]{:S(2)}) async-start(), calls=%async_computation.6 | async-start | bytes 147456 | tf_op jit(solution)/shard_map/reduce_scatter | solution.py:62
  18.1 190.8 %reduce-scatter.11.cloned.1.call-start = ((), (), s32[]{:S(2)}) async-start(), calls=%async_computation.8 | async-start | bytes 294912 | tf_op jit(solution)/shard_map/reduce_scatter | solution.py:64
  19.9 253.7 %reduce-scatter.13.cloned.1.call-start = ((), (), s32[]{:S(2)}) async-start(), calls=%async_computation.9 | async-start | bytes 294912 | tf_op jit(solution)/shard_map/reduce_scatter | solution.py:65
  22.2 303.0 %reduce-scatter.15.cloned.1.call-start = ((), (), s32[]{:S(2)}) async-start(), calls=%async_computation.10 | async-start | bytes 163840 | tf_op jit(solution)/shard_map/reduce_scatter | solution.py:95
  213.9 4.1 copy-start.1
  213.9 59.7 %copy-start.4 = (f32[1024]{0:T(1024)S(1)}, f32[1024]{0:T(1024)}, u32[]{:S(2)}) copy-start(f32[1024]{0:T(1024)} %param.21) | copy-start | bytes 12292
  213.9 91.4 %copy-start.2 = (bf16[1024,512]{1,0:T(8,128)(2,1)S(1)}, bf16[1024,512]{1,0:T(8,128)(2,1)}, u32[]{:S(2)}) copy-start(bf16[1024,512]{1,0:T(8,128)(2,1)} %param.22) | copy-start | bytes 3145732
  213.9 111.2 %copy-start.3 = (bf16[32,512]{1,0:T(8,128)(2,1)S(1)}, bf16[32,512]{1,0:T(8,128)(2,1)}, u32[]{:S(2)}) copy-start(bf16[32,512]{1,0:T(8,128)(2,1)} %param.13) | copy-start | bytes 98308
  213.9 117.4 %copy-start.5 = (f32[512]{0:T(512)S(1)}, f32[512]{0:T(512)}, u32[]{:S(2)}) copy-start(f32[512]{0:T(512)} %param.23) | copy-start | bytes 6148
  306.3 153.8 %all-gather.3.cloned.1.call-start = ((), (), s32[]{:S(2)}) async-start(), calls=%async_computation.12 | async-start | bytes 9437184 | tf_op jit(solution)/shard_map/all_gather | solution.py:108
  335.4 151.3 %reduce-scatter.17.cloned.1.call-start = ((), (), s32[]{:S(2)}) async-start(), calls=%async_computation.11 | async-start | bytes 163840 | tf_op jit(solution)/shard_map/reduce_scatter | solution.py:111
Sparse Core Ops, SparseCore 0:
  16.2 63.4 reduce-scatter.8
  83.0 60.8 reduce-scatter.6
  147.8 61.0 reduce-scatter.10
  212.1 61.4 reduce-scatter.12
  306.5 18.6 reduce-scatter.14
  335.5 124.5 all-gather.2
  468.8 17.8 reduce-scatter.16
